TPU v7x, 32 devices: a whole 2x2x4 slice. The times are simulated.
32 devices in a mesh: rep: 2 (over x), fs: 8 (over z, y), tp: 2 (over core).
Axes of the slice: x: 2, y: 2, z: 4, core: 2. Of those that a mesh axis runs over, the one named last changes fastest.
Arguments:
- tokens: bfloat16 [16, 256, 1024], P(('rep', 'fs'), None, 'tp'), may hold values from -6 to 6
- pre_gain: float32 [1024], replicated, may hold values from 0.1 to 1.9
- first_gate: bfloat16 [1024, 2560], P('fs', 'tp'), may hold values from -0.1875 to 0.1875
- first_up: bfloat16 [1024, 2560], P('fs', 'tp'), may hold values from -0.1875 to 0.1875
- first_down: bfloat16 [2560, 1024], P('tp', 'fs'), may hold values from -0.125 to 0.125
- mix_gain: float32 [1024], P('tp'), may hold values from 0.1 to 1.9
- pool_weight: bfloat16 [4, 256, 256], P('tp', None, 'fs'), may hold values from -0.375 to 0.375
- pool_scale: float32 [1024], P('tp'), may hold values from 0.1 to 1.9
- post_gain: float32 [1024], replicated, may hold values from 0.1 to 1.9
- second_gate: bfloat16 [1024, 2560], P('fs', 'tp'), may hold values from -0.1875 to 0.1875
- second_up: bfloat16 [1024, 2560], P('fs', 'tp'), may hold values from -0.1875 to 0.1875
- second_down: bfloat16 [2560, 1024], P('tp', 'fs'), may hold values from -0.125 to 0.125
Outputs:
- layer_out: bfloat16 [16, 256, 1024], P(('rep', 'fs'), None, 'tp')
All inputs are finite; a program needn't handle non-finite values.
Results may differ from a plain program's by a relative error of at most 0.015.
Values may be sent and summed in bfloat16 or wider, within the bound.
A program may use at most 64 MiB of HBM per device.

v0:
```python
import jax
import jax.numpy as jnp
from jax import lax
from jax.sharding import PartitionSpec as P

D = 1024
GROUPS = 4


epsilon = 1e-06


def taken_in(shard, axis, dim, take_in, carry):
    whole = jax.tree.map(lambda part: lax.all_gather(part, axis, axis=dim, tiled=True), shard)
    return take_in(carry, whole, jnp.int32(0))


def over_all(shard, axis, dim, block):
    whole = lax.all_gather(shard, axis, axis=dim, tiled=True)
    return block(whole, jnp.int32(0))


def normalize(values, gain_vec):
    floats = values.astype(jnp.float32)
    scaled = floats * lax.rsqrt(jnp.mean(floats * floats, axis=-1, keepdims=True) + epsilon)
    return (scaled * gain_vec.astype(jnp.float32)).astype(jnp.bfloat16)


def half_step(local_part, gain_vec, gate_w, up_w, down_w):
    gathered = lax.all_gather(local_part, "tp", axis=2, tiled=True)
    seq_count, seq_length, full_width = gathered.shape
    normed = normalize(gathered.reshape(seq_count * seq_length, full_width), gain_vec)
    zero_init = jnp.zeros((normed.shape[0], gate_w.shape[1]), jnp.float32)

    def add_rows(running, block_rows, offset):
        columns = lax.dynamic_slice_in_dim(normed, offset, block_rows.shape[0], 1)
        return running + jnp.dot(columns, block_rows, preferred_element_type=jnp.float32)

    gate_sum = taken_in(gate_w, "fs", 0, add_rows, zero_init)
    up_sum = taken_in(up_w, "fs", 0, add_rows, zero_init)
    hidden = (jax.nn.silu(gate_sum) * up_sum).astype(jnp.bfloat16)

    def project(block_cols, offset):
        return jnp.dot(hidden, block_cols, preferred_element_type=jnp.float32)

    partial_value = over_all(down_w, "fs", 1, project)
    own_part = lax.psum_scatter(
        partial_value.astype(jnp.bfloat16), "tp", scatter_dimension=1, tiled=True
    ).astype(jnp.float32)
    return own_part.reshape(seq_count, seq_length, own_part.shape[1])


def trailing(grouped, windows, widest):
    seq_length = grouped.shape[1]
    running = jnp.zeros_like(grouped)
    for back_step in range(widest):
        moved = jnp.pad(grouped, ((0, 0), (back_step, 0), (0, 0), (0, 0)))[:, :seq_length]
        running = running + jnp.where(back_step < windows[None, None, :, None], moved, 0.0)
    positions = jnp.arange(seq_length, dtype=jnp.int32)
    counts = jnp.minimum(positions[:, None] + 1, windows[None, :]).astype(jnp.float32)
    return running / counts[None, :, :, None]


def pool_mix(local_part, mix_gain, pool_weight, pool_scale):
    floats = local_part.astype(jnp.float32)
    squares = lax.psum(jnp.sum(floats * floats, axis=-1).astype(jnp.bfloat16), "tp").astype(
        jnp.float32
    )
    normed = (
        floats * lax.rsqrt(squares[..., None] / D + epsilon) * mix_gain.astype(jnp.float32)
    ).astype(jnp.bfloat16)
    seq_count, seq_length, part_width = local_part.shape
    groups_here = pool_weight.shape[0]
    group_width = pool_weight.shape[1]
    grouped = normed.astype(jnp.float32).reshape(seq_count, seq_length, groups_here, group_width)
    group_ids = lax.axis_index("tp") * groups_here + jnp.arange(groups_here, dtype=jnp.int32)
    windows = 2 ** (group_ids + 1)
    pooled = trailing(grouped, windows, 2**GROUPS)
    diff = (pooled - grouped).astype(jnp.bfloat16)

    def mix_cols(block_cols, offset):
        return jnp.einsum("bsgc,gcd->bsgd", diff, block_cols, preferred_element_type=jnp.float32)

    mixed = over_all(pool_weight, "fs", 2, mix_cols)
    mixed = mixed.reshape(seq_count, seq_length, part_width)
    return (floats + mixed * pool_scale.astype(jnp.float32)).astype(jnp.bfloat16)


def local(
    tokens,
    pre_gain,
    first_gate,
    first_up,
    first_down,
    mix_gain,
    pool_weight,
    pool_scale,
    post_gain,
    second_gate,
    second_up,
    second_down,
):
    first_out = half_step(tokens, pre_gain, first_gate, first_up, first_down)
    after_first = (tokens.astype(jnp.float32) + 0.5 * first_out).astype(jnp.bfloat16)
    after_mix = pool_mix(after_first, mix_gain, pool_weight, pool_scale)
    second_out = half_step(after_mix, post_gain, second_gate, second_up, second_down)
    return (after_mix.astype(jnp.float32) + 0.5 * second_out).astype(jnp.bfloat16)


def solution(mesh):
    placed = (
        P(("rep", "fs"), None, "tp"),
        P(),
        P("fs", "tp"),
        P("fs", "tp"),
        P("tp", "fs"),
        P("tp"),
        P("tp", None, "fs"),
        P("tp"),
        P(),
        P("fs", "tp"),
        P("fs", "tp"),
        P("tp", "fs"),
    )
    return jax.shard_map(
        local, mesh=mesh, in_specs=placed, out_specs=P(("rep", "fs"), None, "tp"), check_vma=False
    )
```

profile of v0, /device:TPU:0, one launch (start us, length us, event | category | flops | bytes accessed | tf_op | source)
XLA Modules:
  0.0 382.0 jit_solution(15731106922795846146)
XLA Ops:
  6.5 0.0 all-gather.7.cloned.1.call-start
  6.5 0.7 all-gather.7.cloned.1.call-update
  7.3 0.0 all-gather.11.cloned.1.call-start
  7.3 0.7 all-gather.11.cloned.1.call-update
  8.0 0.0 all-gather.9.cloned.1.call-start
  8.1 0.7 all-gather.9.cloned.1.call-update
  8.7 0.0 reduce-scatter.3.cloned.1.call-start
  8.8 2.5 all_gather.27
  11.3 0.2 fusion.2
  11.5 55.1 %all-gather.7.cloned.1.call-done = bf16[1024,1280]{1,0:T(8,128)(2,1)} async-done(((bf16[128,1280]{1,0:T(8,128)(2,1)}), bf16[1024,1280]{1,0:T(8,128)(2,1)}) %all-gather.7.cloned.1.call-update) | async-done | bytes 2621456 | tf_op jit(solution)/shard_map/all_gather | solution.py:14
  66.7 2.6 fusion.55
  69.3 0.0 copy-start.2
  69.3 0.0 copy-start
  69.4 0.0 copy-start.5
  69.4 54.8 %all-gather.11.cloned.1.call-done = bf16[1280,1024]{1,0:T(8,128)(2,1)} async-done(((bf16[1280,128]{1,0:T(8,128)(2,1)}), bf16[1280,1024]{1,0:T(8,128)(2,1)}) %all-gather.11.cloned.1.call-update) | async-done | bytes 2621456 | tf_op jit(solution)/shard_map/all_gather | solution.py:19
  124.2 55.0 %all-gather.9.cloned.1.call-done = bf16[1024,1280]{1,0:T(8,128)(2,1)} async-done(((bf16[128,1280]{1,0:T(8,128)(2,1)}), bf16[1024,1280]{1,0:T(8,128)(2,1)}) %all-gather.9.cloned.1.call-update) | async-done | bytes 2621456 | tf_op jit(solution)/shard_map/all_gather | solution.py:14
  179.2 0.0 copy-done.3
  179.2 5.0 %convolution_convert_fusion.1 = bf16[256,1024]{1,0:T(8,128)(2,1)} fusion(bf16[1280,1024]{1,0:T(8,128)(2,1)} %all-gather.11.cloned.1.call-done, bf16[1024,1280]{1,0:T(8,128)(2,1)} %all-gather.9.cloned.1.call-done, f32[256,1280]{1,0:T(8,128)S(1)} %fusion.55, bf16[1,256,1024]{2,1,0:T(8,128)(2,1)S(1)} %all_gather.27, f32[1024]{0:T(1024)S(1)} %copy-done.3, ...), kind=kOutput, calls=%fused_computation.9 | convolution fusion | flops 1345454080 | bytes 7607296 | tf_op jit(solution)/shard_map/dot_general | solution.py:44
  184.2 0.0 reduce-scatter.3.cloned.1.call-update
  184.2 0.0 all-gather.13.cloned.1.call-start
  184.3 0.5 all-gather.13.cloned.1.call-update
  184.8 0.0 all-gather.15.cloned.1.call-start
  184.9 0.5 all-gather.15.cloned.1.call-update
  185.4 0.0 all-gather.17.cloned.1.call-start
  185.4 0.7 all-gather.17.cloned.1.call-update
  186.1 0.0 reduce-scatter.5.cloned.1.call-start
  186.4 0.0 copy-done.2
  186.4 31.4 %all_gather.31 = bf16[2,256,256]{1,2,0:T(8,128)(2,1)S(1)} all-gather(bf16[2,256,32]{1,2,0:T(8,128)(2,1)S(1)} %copy-done.2), channel_id=1, replica_groups=mesh['rep'=2,'fs'=8,'tp'=2] {'fs'}, dimensions={2}, use_global_device_ids=true | all-gather | bytes 294912 | tf_op jit(solution)/shard_map/all_gather | solution.py:19
  217.8 0.1 minimum_convert_fusion
  217.9 1.1 fusion.40
  219.0 2.5 psum.7
  221.5 0.0 copy-done.5
  221.5 1.1 fusion.46
  222.7 0.0 copy-start.6
  222.7 1.8 fusion.47
  224.5 0.0 copy-start.4
  224.5 0.2 copy.31
  224.7 0.1 fusion.43
  224.8 2.2 all_gather.32
  227.0 0.2 fusion.5
  227.2 21.9 %all-gather.13.cloned.1.call-done = bf16[1024,1280]{1,0:T(8,128)(2,1)} async-done(((bf16[128,1280]{1,0:T(8,128)(2,1)}), bf16[1024,1280]{1,0:T(8,128)(2,1)}) %all-gather.13.cloned.1.call-update) | async-done | bytes 2621456 | tf_op jit(solution)/shard_map/all_gather | solution.py:14
  249.1 2.6 fusion.51
  251.7 52.7 %all-gather.15.cloned.1.call-done = bf16[1024,1280]{1,0:T(8,128)(2,1)} async-done(((bf16[128,1280]{1,0:T(8,128)(2,1)}), bf16[1024,1280]{1,0:T(8,128)(2,1)}) %all-gather.15.cloned.1.call-update) | async-done | bytes 2621456 | tf_op jit(solution)/shard_map/all_gather | solution.py:14
  304.4 57.5 %all-gather.17.cloned.1.call-done = bf16[1280,1024]{1,0:T(8,128)(2,1)} async-done(((bf16[1280,128]{1,0:T(8,128)(2,1)}), bf16[1280,1024]{1,0:T(8,128)(2,1)}) %all-gather.17.cloned.1.call-update) | async-done | bytes 2621456 | tf_op jit(solution)/shard_map/all_gather | solution.py:19
  361.9 5.0 %convolution_convert_fusion = bf16[256,1024]{1,0:T(8,128)(2,1)} fusion(bf16[1280,1024]{1,0:T(8,128)(2,1)} %all-gather.17.cloned.1.call-done, bf16[1024,1280]{1,0:T(8,128)(2,1)} %all-gather.15.cloned.1.call-done, f32[256,1280]{1,0:T(8,128)S(1)} %fusion.51, bf16[1,256,1024]{2,1,0:T(8,128)(2,1)S(1)} %all_gather.32, f32[1024]{0:T(1024)S(1)} %copy-done.4, ...), kind=kOutput, calls=%fused_computation.8 | convolution fusion | flops 1345454080 | bytes 7607296 | tf_op jit(solution)/shard_map/dot_general | solution.py:44
  366.9 0.0 reduce-scatter.5.cloned.1.call-update
  367.0 6.5 %reduce-scatter.5.cloned.1.call-done = bf16[256,512]{1,0:T(8,128)(2,1)} async-done(((bf16[256,1024]{1,0:T(8,128)(2,1)}), bf16[256,512]{1,0:T(8,128)(2,1)}) %reduce-scatter.5.cloned.1.call-update) | async-done | bytes 262160 | tf_op jit(solution)/shard_map/reduce_scatter | solution.py:47
  373.4 1.7 fusion.44
  (22 shorter events, 0.2 us)
Async XLA Ops:
  6.5 60.1 %all-gather.7.cloned.1.call-start = ((), (), s32[]{:S(2)}) async-start(), calls=%async_computation.2 | async-start | bytes 2949120 | tf_op jit(solution)/shard_map/all_gather | solution.py:14
  7.3 117.0 %all-gather.11.cloned.1.call-start = ((), (), s32[]{:S(2)}) async-start(), calls=%async_computation.4 | async-start | bytes 2949120 | tf_op jit(solution)/shard_map/all_gather | solution.py:19
  8.0 171.2 %all-gather.9.cloned.1.call-start = ((), (), s32[]{:S(2)}) async-start(), calls=%async_computation.3 | async-start | bytes 2949120 | tf_op jit(solution)/shard_map/all_gather | solution.py:14
  8.7 209.2 %reduce-scatter.3.cloned.1.call-start = ((), (), s32[]{:S(2)}) async-start(), calls=%async_computation.5 | async-start | bytes 786432 | tf_op jit(solution)/shard_map/reduce_scatter | solution.py:47
  11.3 167.9 %copy-start.3 = (f32[1024]{0:T(1024)S(1)}, f32[1024]{0:T(1024)}, u32[]{:S(2)}) copy-start(f32[1024]{0:T(1024)} %param.13) | copy-start | bytes 12292
  69.3 117.1 %copy-start.2 = (bf16[2,256,32]{1,2,0:T(8,128)(2,1)S(1)}, bf16[2,256,32]{1,2,0:T(8,128)(2,1)}, u32[]{:S(2)}) copy-start(bf16[2,256,32]{1,2,0:T(8,128)(2,1)} %param.18) | copy-start | bytes 98308
  69.3 148.6 %copy-start = (bf16[1,256,512]{2,1,0:T(8,128)(2,1)S(1)}, bf16[1,256,512]{2,1,0:T(8,128)(2,1)}, u32[]{:S(2)}) copy-start(bf16[1,256,512]{2,1,0:T(8,128)(2,1)} %param.12) | copy-start | bytes 786436
  69.4 152.2 %copy-start.5 = (f32[512]{0:T(512)S(1)}, f32[512]{0:T(512)}, u32[]{:S(2)}) copy-start(f32[512]{0:T(512)} %param.17) | copy-start | bytes 6148
  184.2 64.9 %all-gather.13.cloned.1.call-start = ((), (), s32[]{:S(2)}) async-start(), calls=%async_computation.6 | async-start | bytes 2949120 | tf_op jit(solution)/shard_map/all_gather | solution.py:14
  184.8 119.6 %all-gather.15.cloned.1.call-start = ((), (), s32[]{:S(2)}) async-start(), calls=%async_computation.7 | async-start | bytes 2949120 | tf_op jit(solution)/shard_map/all_gather | solution.py:14
  185.4 176.6 %all-gather.17.cloned.1.call-start = ((), (), s32[]{:S(2)}) async-start(), calls=%async_computation.8 | async-start | bytes 2949120 | tf_op jit(solution)/shard_map/all_gather | solution.py:19
  186.1 187.3 %reduce-scatter.5.cloned.1.call-start = ((), (), s32[]{:S(2)}) async-start(), calls=%async_computation.9 | async-start | bytes 786432 | tf_op jit(solution)/shard_map/reduce_scatter | solution.py:47
  222.6 2.0 copy-start.1
  222.7 2.0 copy-start.6
  224.5 24.6 %copy-start.4 = (f32[1024]{0:T(1024)S(1)}, f32[1024]{0:T(1024)}, u32[]{:S(2)}) copy-start(f32[1024]{0:T(1024)} %param.20) | copy-start | bytes 12292
Sparse Core Ops, SparseCore 0:
  9.5 57.1 all-gather.6
  68.7 55.4 all-gather.10
  126.4 52.7 all-gather.8
  184.3 6.7 reduce-scatter.2
  193.2 55.8 all-gather.12
  251.1 53.2 all-gather.14
  306.4 55.4 all-gather.16
  367.1 6.2 reduce-scatter.4
where the time goes:
time: 382 us
  waiting for transfers between devices  307 us (80%)
  blocking collectives  38.6 us (10%)
  matrix products  17.1 us (4%)
  between operations  13.7 us (4%)
  other arithmetic  4.68 us (1%)
    all_gather x4, waiting for transfers between devices, taken_in(): lax.all_gather(part, axis, axis=dim, tiled=True)  185 us
    all_gather x2, waiting for transfers between devices, over_all(): whole = lax.all_gather(shard, axis, axis=dim, tiled=True)  112 us
    all_gather x1, blocking collectives, over_all(): whole = lax.all_gather(shard, axis, axis=dim, tiled=True)  31.4 us
    dot_general x2, matrix products, project(): return jnp.dot(hidden, block_cols, preferred_element_type=jnp.float32)  10 us
  transfers between devices with their start and end apart: 8, of which 7 were waited for; matrix products, arithmetic and copies ran while one was open for 3% of the time, Pallas kernels for 0%

commit v1 on v0

--- a/solution.py
+++ b/solution.py
@@ -1,6 +1,10 @@
+import functools
+
 import jax
 import jax.numpy as jnp
 from jax import lax
+from jax.experimental import pallas as pl
+from jax.experimental.pallas import tpu as pltpu
 from jax.sharding import PartitionSpec as P
 
 D = 1024
@@ -107,6 +111,431 @@
     return (after_mix.astype(jnp.float32) + 0.5 * second_out).astype(jnp.bfloat16)
 
 
+F32 = jnp.float32
+BF16 = jnp.bfloat16
+
+
+def layer_kernel(
+    nz, tok_ref, pre_ref, mixg_ref, scale_ref, post_ref, pw_ref, tail1_ref, tail2_ref,
+    g1_ref, u1_ref, d1_ref, g2_ref, u2_ref, d2_ref, out_ref,
+    GU, DW, PW, T, N, ACC, H, PS, PR, S, R, SQ,
+    sw_s, sw_r, loc, zs, zr, ts, tr, cs, cr, os_, or_, ps_, pr_, qs, qr,
+):
+    r = lax.axis_index("rep")
+    f = lax.axis_index("fs")
+    t = lax.axis_index("tp")
+    x = lax.rem(r, 2)
+    y = lax.rem(f, 2)
+    z = f // 2
+    rx = r + 1 - 2 * x
+    fy = f + 1 - 2 * y
+    me = 2 * x + y
+    other = 1 - t
+
+    def dev(rr, ff, tt):
+        return {"rep": rr, "fs": ff, "tp": tt}
+
+    quad = (dev(rx, f, t), dev(r, fy, t), dev(rx, fy, t))
+    quad_idx = (2 * (1 - x) + y, 2 * x + (1 - y), 2 * (1 - x) + (1 - y))
+    mate = dev(r, f, other)
+    above = dev(r, f + 2, t)
+    below = dev(r, f - 2, t)
+    has_above = z < nz - 1
+    has_below = z > 0
+
+    barrier = pltpu.get_barrier_semaphore()
+    for peer in quad + (mate,):
+        pl.semaphore_signal(barrier, inc=1, device_id=peer, device_id_type=pl.DeviceIdType.MESH)
+
+    @pl.when(has_above)
+    def _():
+        pl.semaphore_signal(barrier, inc=1, device_id=above, device_id_type=pl.DeviceIdType.MESH)
+
+    @pl.when(has_below)
+    def _():
+        pl.semaphore_signal(barrier, inc=1, device_id=below, device_id_type=pl.DeviceIdType.MESH)
+
+    def remote(src, dst, ss, rs, to):
+        return pltpu.make_async_remote_copy(
+            src_ref=src, dst_ref=dst, send_sem=ss, recv_sem=rs,
+            device_id=to, device_id_type=pl.DeviceIdType.MESH,
+        )
+
+    rows, half = tok_ref.shape
+    depth = g1_ref.shape[0]
+    main = (g1_ref.shape[1] // 512) * 128
+    rest = g1_ref.shape[1] // 4 - main
+    big = GU.shape[-1]
+    cw = d1_ref.shape[1]
+    weights = ((g1_ref, u1_ref, tail1_ref, d1_ref), (g2_ref, u2_ref, tail2_ref, d2_ref))
+
+    def pieces(b, q):
+        g, u, tl, d = weights[b]
+        lanes = pl.ds(pl.multiple_of(q * main, 128), main)
+        ends = pl.ds(pl.multiple_of(q * 2 * rest, 128), 2 * rest)
+        deep = pl.ds(pl.multiple_of(y * depth, 128), depth)
+        rows_main = pl.ds(pl.multiple_of(q * main, 128), main)
+        rows_rest = pl.ds(pl.multiple_of(4 * main + q * rest, 16), rest)
+        return (
+            (g.at[:, lanes], GU.at[b, z, deep, 0:main]),
+            (u.at[:, lanes], GU.at[b, z, deep, main:2 * main]),
+            (tl.at[:, ends], GU.at[b, z, deep, 2 * main:big]),
+            (d.at[rows_main, :], DW.at[b, z, y, 0:main, :]),
+            (d.at[rows_rest, :], DW.at[b, z, y, main:main + rest, :]),
+        )
+
+    def own_copies(b):
+        found = [pltpu.make_async_copy(s, d, loc.at[b, i]) for i, (s, d) in enumerate(pieces(b, me))]
+        if b == 0:
+            found.append(pltpu.make_async_copy(pw_ref, PW.at[z, y], loc.at[b, 5]))
+        return found
+
+    def swaps(b):
+        found = [
+            remote(s, d, sw_s.at[b, i], sw_r.at[b, i], quad[1])
+            for i, (s, d) in enumerate(pieces(b, quad_idx[1]))
+        ]
+        if b == 0:
+            found.append(remote(pw_ref, PW.at[z, y], sw_s.at[b, 5], sw_r.at[b, 5], quad[1]))
+        return found
+
+    kinds = (GU, DW)
+
+    def z_up(b, k, kind):
+        p = jnp.maximum(z - k, 0)
+        ref = PW.at[p] if kind == 2 else kinds[kind].at[b, p]
+        return remote(ref, ref, zs.at[0, b, k, kind], zr.at[0, b, k, kind], above)
+
+    def z_down(b, k, kind):
+        p = jnp.minimum(z + k, nz - 1)
+        ref = PW.at[p] if kind == 2 else kinds[kind].at[b, p]
+        return remote(ref, ref, zs.at[1, b, k, kind], zr.at[1, b, k, kind], below)
+
+    def can_up(k):
+        return jnp.logical_and(has_above, z - k >= 0)
+
+    def can_down(k):
+        return jnp.logical_and(has_below, z + k <= nz - 1)
+
+    def z_send(b, k, kind):
+        @pl.when(can_up(k))
+        def _():
+            z_up(b, k, kind).start()
+
+        @pl.when(can_down(k))
+        def _():
+            z_down(b, k, kind).start()
+
+    def z_sent(b, k, kind):
+        @pl.when(can_up(k))
+        def _():
+            z_up(b, k, kind).wait_send()
+
+        @pl.when(can_down(k))
+        def _():
+            z_down(b, k, kind).wait_send()
+
+    def z_take(b, k, kind):
+        @pl.when(z - 1 - k >= 0)
+        def _():
+            z_up(b, k, kind).wait_recv()
+
+        @pl.when(z + 1 + k <= nz - 1)
+        def _():
+            z_down(b, k, kind).wait_recv()
+
+        if k + 1 < nz - 1:
+            z_send(b, k + 1, kind)
+
+    def tok_sends(b):
+        mine = T.at[b, me, t]
+        return [remote(mine, mine, ts.at[b, j], tr.at[b, j], quad[j]) for j in range(3)]
+
+    def mate_own(b):
+        mine = T.at[b, me, t]
+        return remote(mine, mine, os_.at[b], or_.at[b], mate)
+
+    def mate_pass(b, j):
+        got = T.at[b, quad_idx[j], t]
+        return remote(got, got, cs.at[b, j], cr.at[b, j], mate)
+
+    def order(i):
+        m = jnp.minimum(z, nz - 1 - z)
+        near = z - (i + 1) // 2 if i % 2 else z + i // 2
+        far = jnp.where(2 * z < nz - 1, i, nz - 1 - i)
+        return jnp.where(i <= 2 * m, near, far)
+
+    def norm_block(b, q, gain_ref):
+        parts = [T[b, q, c].astype(F32) for c in range(2)]
+        total = sum(jnp.sum(v * v, axis=-1, keepdims=True) for v in parts)
+        inv = lax.rsqrt(total / (2 * half) + epsilon)
+        step = N.shape[2]
+        for c in range(2):
+            done = (parts[c] * inv * gain_ref[0:1, c * half:(c + 1) * half]).astype(BF16)
+            for i in range(half // step):
+                N[c * (half // step) + i, pl.ds(pl.multiple_of(q * rows, 128), rows), :] = done[:, i * step:(i + 1) * step]
+
+    def gate_up(b, i):
+        p = order(i)
+
+        @pl.loop(0, 4)
+        def _(q):
+            at = pl.ds(pl.multiple_of(q * rows, 128), rows)
+            value = jnp.dot(N[p, at, :], GU[b, p], preferred_element_type=F32)
+            if i == 0:
+                ACC[at, :] = value
+            else:
+                ACC[at, :] += value
+
+    def hidden_of():
+        @pl.loop(0, 4)
+        def _(q):
+            at = pl.ds(pl.multiple_of(q * rows, 128), rows)
+            gate = ACC[at, 0:main]
+            up = ACC[at, main:2 * main]
+            H[at, 0:main] = (jax.nn.silu(gate) * up).astype(BF16)
+            last = ACC[at, 2 * main:big]
+            H[at, main:main + rest] = (jax.nn.silu(last[:, :rest]) * last[:, rest:]).astype(BF16)
+
+    def half_sends(b):
+        span = pl.ds(other * (nz // 2), nz // 2)
+        return [
+            remote(
+                PS.at[b, q, span], PR.at[b, q], ps_.at[b, q], pr_.at[b, q], mate
+            )
+            for q in range(4)
+        ]
+
+    def down(b):
+        sends = half_sends(b)
+        for q in range(4):
+            for p in range(nz):
+                wide = jnp.concatenate([DW[b, p, 0], DW[b, p, 1]], axis=1)
+                PS[b, q, p] = jnp.dot(
+                    H[q * rows:(q + 1) * rows, :], wide, preferred_element_type=F32
+                ).astype(BF16)
+            sends[q].start()
+
+    def sum_half(b, q):
+        for i in range(nz // 2):
+            mine = PS[b, q, t * (nz // 2) + i].astype(F32)
+            S[b, q, :, i * 2 * cw:(i + 1) * 2 * cw] = (mine + PR[b, q, i].astype(F32)).astype(BF16)
+
+    def quad_sends(b):
+        return [
+            remote(S.at[b, quad_idx[j]], R.at[b, j], qs.at[b, j], qr.at[b, j], quad[j])
+            for j in range(3)
+        ]
+
+    def scatter(b):
+        sends = half_sends(b)
+        for q in range(4):
+            sends[q].wait_recv()
+            sum_half(b, q)
+        for j in (2, 1, 0):
+            quad_sends(b)[j].start()
+
+    def collect(b):
+        for send in quad_sends(b):
+            send.wait_recv()
+        total = S[b, me].astype(F32)
+        for j in range(3):
+            total = total + R[b, j].astype(F32)
+        return total
+
+    for c in own_copies(0):
+        c.start()
+    T[0, me, t] = tok_ref[...]
+    pl.semaphore_wait(
+        barrier, 4 + jnp.minimum(z, 1) + jnp.minimum(nz - 1 - z, 1)
+    )
+
+    for c in swaps(0)[:5]:
+        c.start()
+    for j in (0, 2, 1):
+        tok_sends(0)[j].start()
+    mate_own(0).start()
+    swaps(0)[5].start()
+    for c in own_copies(1):
+        c.start()
+    for c in swaps(1):
+        c.start()
+    for i, c in enumerate(own_copies(0)):
+        c.wait()
+    for i in (0, 1, 2):
+        swaps(0)[i].wait_recv()
+    z_send(0, 0, 0)
+    for i in (3, 4):
+        swaps(0)[i].wait_recv()
+    z_send(0, 0, 1)
+    mate_own(0).wait_recv()
+    norm_block(0, me, pre_ref)
+    for j in (0, 2, 1):
+        tok_sends(0)[j].wait_recv()
+        mate_pass(0, j).start()
+    for j in (0, 2, 1):
+        mate_pass(0, j).wait_recv()
+        norm_block(0, quad_idx[j], pre_ref)
+    swaps(0)[5].wait_recv()
+    gate_up(0, 0)
+    for k in range(nz - 1):
+        z_take(0, k, 0)
+        gate_up(0, k + 1)
+        z_take(0, k, 1)
+        if k == 0:
+            z_send(0, 0, 2)
+        else:
+            z_take(0, k - 1, 2)
+        if k == max(nz - 3, 0):
+            for c in own_copies(1):
+                c.wait()
+            for c in swaps(1):
+                c.wait_recv()
+            z_send(1, 0, 0)
+            z_send(1, 0, 1)
+    hidden_of()
+    down(0)
+    scatter(0)
+    z_take(0, nz - 2, 2)
+    z_take(1, 0, 0)
+    z_take(1, 0, 1)
+    first = collect(0)
+    after_first = (tok_ref[...].astype(F32) + 0.5 * first).astype(BF16).astype(F32)
+    square = after_first * after_first
+    SQ[0] = sum(square[:, i * 128:(i + 1) * 128] for i in range(half // 128))
+    swap_sq = remote(SQ.at[0], SQ.at[1], os_.at[2], or_.at[2], mate)
+    swap_sq.start()
+    swap_sq.wait_recv()
+    total = jnp.sum(SQ[0] + SQ[1], axis=-1, keepdims=True)
+    h = (after_first * lax.rsqrt(total / (2 * half) + epsilon) * mixg_ref[0:1, :]).astype(BF16).astype(F32)
+    position = lax.broadcasted_iota(jnp.int32, (rows, 128), 0)
+    groups_here = pw_ref.shape[0]
+    width = half // groups_here
+
+    def shifted(v, by):
+        place = lax.broadcasted_iota(jnp.int32, v.shape, 0)
+        return jnp.where(place >= by, pltpu.roll(v, by, 0), 0.0)
+
+    for g in range(groups_here):
+        hg = h[:, g * width:(g + 1) * width]
+        run = hg + shifted(hg, 1)
+        window = 2
+        found = run
+        number = t * groups_here + g
+        reached = jnp.int32(2)
+        for level in range(1, GROUPS):
+            run = run + shifted(run, window)
+            window = window * 2
+            found = jnp.where(number >= level, run, found)
+            reached = jnp.where(number >= level, window, reached)
+        counts = jnp.minimum(lax.broadcasted_iota(jnp.int32, (rows, width), 0) + 1, reached).astype(F32)
+        diff = (found / counts - hg).astype(BF16)
+        turned = jnp.concatenate([PW[i // 2, i % 2, g] for i in range(2 * nz)], axis=0)
+        mixed = lax.dot_general(diff, turned, (((1,), (1,)), ((), ())), preferred_element_type=F32)
+        at = slice(g * width, (g + 1) * width)
+        T[1, me, t, :, at] = (after_first[:, at] + scale_ref[0:1, at] * mixed).astype(BF16)
+    for j in (0, 2, 1):
+        tok_sends(1)[j].start()
+    mate_own(1).start()
+    z_take(1, 1, 0)
+    z_take(1, 1, 1)
+    mate_own(1).wait_recv()
+    norm_block(1, me, post_ref)
+    for j in (0, 2, 1):
+        tok_sends(1)[j].wait_recv()
+        mate_pass(1, j).start()
+    for j in (0, 2, 1):
+        mate_pass(1, j).wait_recv()
+        norm_block(1, quad_idx[j], post_ref)
+    for i in range(nz - 1):
+        gate_up(1, i)
+    for k in range(2, nz - 1):
+        z_take(1, k, 0)
+        z_take(1, k, 1)
+    gate_up(1, nz - 1)
+    hidden_of()
+    down(1)
+    scatter(1)
+    out_ref[...] = (T[1, me, t].astype(F32) + 0.5 * collect(1)).astype(BF16)
+
+    for b in range(2):
+        for c in swaps(b) + tok_sends(b) + [mate_own(b)] + [mate_pass(b, j) for j in range(3)]:
+            c.wait_send()
+        for c in half_sends(b) + quad_sends(b):
+            c.wait_send()
+        for k in range(nz - 1):
+            for kind in range(3 if b == 0 else 2):
+                z_sent(b, k, kind)
+    swap_sq.wait_send()
+
+
+def fused(
+    fs, tokens, pre_gain, first_gate, first_up, first_down, mix_gain, pool_weight,
+    pool_scale, post_gain, second_gate, second_up, second_down,
+):
+    nz = fs // 2
+    _, rows, half = tokens.shape
+    depth, hid = first_gate.shape
+    cw = first_down.shape[1]
+    main = (hid // 512) * 128
+    rest = hid // 4 - main
+    groups, width, out_cols = pool_weight.shape
+
+    def tail_of(gate, up):
+        parts = [v[:, 4 * main:].reshape(depth, 4, rest) for v in (gate, up)]
+        return jnp.concatenate(parts, axis=2).reshape(depth, 8 * rest)
+
+    vmem = pl.BlockSpec(memory_space=pltpu.VMEM)
+    anyw = pl.BlockSpec(memory_space=pl.ANY)
+    dma = pltpu.SemaphoreType.DMA
+    big = 2 * main + 2 * rest
+    steps = nz - 1
+    out = pl.pallas_call(
+        functools.partial(layer_kernel, nz),
+        out_shape=jax.ShapeDtypeStruct((rows, half), BF16),
+        in_specs=[vmem] * 6 + [anyw] * 8,
+        out_specs=vmem,
+        scratch_shapes=[
+            pltpu.VMEM((2, nz, 2 * depth, big), BF16),
+            pltpu.VMEM((2, nz, 2, main + rest, cw), BF16),
+            pltpu.VMEM((nz, 2, groups, out_cols, width), BF16),
+            pltpu.VMEM((2, 4, 2, rows, half), BF16),
+            pltpu.VMEM((nz, 4 * rows, 2 * depth), BF16),
+            pltpu.VMEM((4 * rows, big), F32),
+            pltpu.VMEM((4 * rows, main + rest), BF16),
+            pltpu.VMEM((2, 4, nz, rows, 2 * cw), BF16),
+            pltpu.VMEM((2, 4, nz // 2, rows, 2 * cw), BF16),
+            pltpu.VMEM((2, 4, rows, half), BF16),
+            pltpu.VMEM((2, 3, rows, half), BF16),
+            pltpu.VMEM((2, rows, 128), F32),
+            dma((2, 6)), dma((2, 6)), dma((2, 6)),
+            dma((2, 2, steps, 3)), dma((2, 2, steps, 3)),
+            dma((2, 3)), dma((2, 3)), dma((2, 3)), dma((2, 3)),
+            dma((3,)), dma((3,)), dma((2, 4)), dma((2, 4)), dma((2, 3)), dma((2, 3)),
+        ],
+        compiler_params=pltpu.CompilerParams(
+            collective_id=0, has_side_effects=True, vmem_limit_bytes=60 * 1024 * 1024
+        ),
+    )(
+        tokens.reshape(rows, half), pre_gain.reshape(1, -1), mix_gain.reshape(1, -1),
+        pool_scale.reshape(1, -1), post_gain.reshape(1, -1), jnp.swapaxes(pool_weight, 1, 2),
+        tail_of(first_gate, first_up), tail_of(second_gate, second_up),
+        first_gate, first_up, first_down, second_gate, second_up, second_down,
+    )
+    return out.reshape(tokens.shape)
+
+
+def whole_tiles(mesh, args):
+    reps, fs, tp = (mesh.shape[name] for name in ("rep", "fs", "tp"))
+    depth = args[2].shape[0] // fs
+    hid = args[2].shape[1] // tp
+    return (
+        tp == 2 and reps % 2 == 0 and fs % 8 == 0 and depth % 128 == 0
+        and args[0].shape[0] == reps * fs and args[4].shape[1] // fs == depth
+        and hid % 512 == 256 and args[6].shape[2] % (fs * 16) == 0
+    )
+
+
 def solution(mesh):
     placed = (
         P(("rep", "fs"), None, "tp"),
@@ -122,6 +551,10 @@
         P("fs", "tp"),
         P("tp", "fs"),
     )
-    return jax.shard_map(
-        local, mesh=mesh, in_specs=placed, out_specs=P(("rep", "fs"), None, "tp"), check_vma=False
-    )
+    def layer(*args):
+        body = functools.partial(fused, mesh.shape["fs"]) if whole_tiles(mesh, args) else local
+        return jax.shard_map(
+            body, mesh=mesh, in_specs=placed, out_specs=P(("rep", "fs"), None, "tp"), check_vma=False
+        )(*args)
+
+    return layer

time: 382 us -> 117 us (0.31)
  waiting for transfers between devices: 307 us -> 0 us
  Pallas kernels: 0 us -> 110 us
  blocking collectives: 38.6 us -> 0 us
  matrix products: 17.1 us -> 0 us
  between operations: 13.7 us -> 0.07 us
  local copies, waits for them, and re-layouts: 0.28 us -> 7 us
  other arithmetic: 4.68 us -> 0.02 us
    all_gather x6 -> x0, waiting for transfers between devices: 297 us -> none  [the longest x4 185 us: taken_in(): lax.all_gather(part, axis, axis=dim, tiled=True)]
    pallas_call x0 -> x1, Pallas kernels: none -> 110 us  [fused(): pl.pallas_call(functools.partial(layer_kernel, nz), out_shape=jax.ShapeDt...]
    all_gather x3 -> x0, blocking collectives: 36.2 us -> none  [the longest x1 31.4 us: over_all(): whole = lax.all_gather(shard, axis, axis=dim, tiled=True)]
    dot_general x5 -> x0, matrix products: 17.1 us -> none  [the longest x2 10 us: project(): return jnp.dot(hidden, block_cols, preferred_element_type=jnp.float32)]
    reduce_scatter x2 -> x0, waiting for transfers between devices: 6.46 us -> none  [half_step(): lax.psum_scatter(partial_value.astype(jnp.bfloat16), 'tp', scatter_dimens...]
    unnamed x8 -> x0, waiting for transfers between devices: 3.87 us -> none
  transfers between devices with their start and end apart: 8 -> 0, of which waited for: 7 -> 0; matrix products, arithmetic and copies ran while one was open for 3% -> 0% of each run, Pallas kernels for 0% -> 0%
where the time goes in v1:
time: 117 us
  Pallas kernels  110 us (94%)
  local copies, waits for them, and re-layouts  7 us (6%)
    pallas_call x1, Pallas kernels, fused(): pl.pallas_call(functools.partial(layer_kernel, nz), out_shape=jax.ShapeDt...  110 us
    slice x8, local copies, waits for them, and re-layouts, tail_of(): parts = [v[:, 4 * main:].reshape(depth, 4, rest) for v in (gate, up)]  3.35 us

profile of v1, /device:TPU:0, one launch (start us, length us, event | category | flops | bytes accessed | tf_op | source)
XLA Modules:
  0.0 116.8 jit_solution(4399160880004494688)
XLA Ops:
  0.0 0.0 slice-start.1
  0.0 0.8 slice-done.1
  0.8 0.1 copy.21
  1.0 0.0 slice-start
  1.0 0.8 slice-done
  1.8 0.1 copy.22
  1.9 0.8 copy.19.tail1_ref
  2.7 0.0 slice-start.3
  2.7 0.8 slice-done.3
  3.5 0.1 copy.23
  3.7 0.0 slice-start.2
  3.7 0.8 slice-done.2
  4.5 0.1 copy.24
  4.6 0.8 copy.20.tail2_ref
  5.4 109.7 %shard_map.118 = bf16[256,512]{1,0:T(8,128)(2,1)} custom-call(bf16[256,512]{1,0:T(8,128)(2,1)} %bitcast.20, f32[1,1024]{1,0:T(1,128)} %bitcast.22, f32[1,512]{1,0:T(1,128)} %bitcast.24, f32[1,512]{1,0:T(1,128)} %bitcast.25, f32[1,1024]{1,0:T(1,128)} %bitcast.23, bf16[2,32,256]{2,1,0:T(8,128)(2,1)} %bitcast.21, bf16[128,512]{1,0:T(8,128)(2,1)} %copy.19.tail1_ref, ...), custom_call_target="tpu_custom_call" | custom-call | tf_op jit(solution)/shard_map/pallas_call | solution.py:493
  115.1 1.7 %copy.26 = bf16[1,256,512]{2,1,0:T(8,128)(2,1)} copy(bf16[1,256,512]{2,1,0:T(8,128)(2,1)} %bitcast.13) | data formatting | bytes 524288
  (2 shorter events, 0.0 us)
Async XLA Ops:
  0.0 0.8 slice-start.1
  1.0 0.8 slice-start
  2.7 0.8 slice-start.3
  3.7 0.8 slice-start.2

commit v2 on v1

--- a/solution.py
+++ b/solution.py
@@ -116,9 +116,9 @@
 
 
 def layer_kernel(
-    nz, tok_ref, pre_ref, mixg_ref, scale_ref, post_ref, pw_ref, tail1_ref, tail2_ref,
+    nz, tok_ref, pre_ref, mixg_ref, scale_ref, post_ref, pw_ref,
     g1_ref, u1_ref, d1_ref, g2_ref, u2_ref, d2_ref, out_ref,
-    GU, DW, PW, T, N, ACC, H, PS, PR, S, R, SQ,
+    GU, DW, PW, T, N, ACC, H, PS, PR, S, R, SQ, TG, TL, tg_s,
     sw_s, sw_r, loc, zs, zr, ts, tr, cs, cr, os_, or_, ps_, pr_, qs, qr,
 ):
     r = lax.axis_index("rep")
@@ -167,7 +167,7 @@
     rest = g1_ref.shape[1] // 4 - main
     big = GU.shape[-1]
     cw = d1_ref.shape[1]
-    weights = ((g1_ref, u1_ref, tail1_ref, d1_ref), (g2_ref, u2_ref, tail2_ref, d2_ref))
+    weights = ((g1_ref, u1_ref, TL.at[0], d1_ref), (g2_ref, u2_ref, TL.at[1], d2_ref))
 
     def pieces(b, q):
         g, u, tl, d = weights[b]
@@ -184,6 +184,21 @@
             (d.at[rows_rest, :], DW.at[b, z, y, main:main + rest, :]),
         )
 
+    def tail_loads(b):
+        return [
+            pltpu.make_async_copy(weights[b][i].at[:, 4 * main:], TG.at[b, i], tg_s.at[b, i])
+            for i in range(2)
+        ]
+
+    def tail_make(b):
+        for c in tail_loads(b):
+            c.wait()
+        for q in range(4):
+            cut = slice(q * rest, (q + 1) * rest)
+            TL[b, :, q * 2 * rest:(q + 1) * 2 * rest] = jnp.concatenate(
+                [TG[b, 0, :, cut], TG[b, 1, :, cut]], axis=1
+            )
+
     def own_copies(b):
         found = [pltpu.make_async_copy(s, d, loc.at[b, i]) for i, (s, d) in enumerate(pieces(b, me))]
         if b == 0:
@@ -287,65 +302,83 @@
             else:
                 ACC[at, :] += value
 
-    def hidden_of():
-        @pl.loop(0, 4)
-        def _(q):
-            at = pl.ds(pl.multiple_of(q * rows, 128), rows)
-            gate = ACC[at, 0:main]
-            up = ACC[at, main:2 * main]
-            H[at, 0:main] = (jax.nn.silu(gate) * up).astype(BF16)
-            last = ACC[at, 2 * main:big]
-            H[at, main:main + rest] = (jax.nn.silu(last[:, :rest]) * last[:, rest:]).astype(BF16)
+    turn = (quad_idx[2], quad_idx[0], quad_idx[1], me)
+    turn_peer = (2, 0, 1)
+
+    def rows_of(q):
+        return pl.ds(pl.multiple_of(q * rows, 128), rows)
+
+    def hidden_of(q):
+        at = rows_of(q)
+        gate = ACC[at, 0:main]
+        up = ACC[at, main:2 * main]
+        H[at, 0:main] = (jax.nn.silu(gate) * up).astype(BF16)
+        last = ACC[at, 2 * main:big]
+        H[at, main:main + rest] = (jax.nn.silu(last[:, :rest]) * last[:, rest:]).astype(BF16)
+
+    def half_send(b, i):
+        span = pl.ds(other * (nz // 2), nz // 2)
+        q = turn[i]
+        return remote(PS.at[b, q, span], PR.at[b, q], ps_.at[b, i], pr_.at[b, i], mate)
 
     def half_sends(b):
-        span = pl.ds(other * (nz // 2), nz // 2)
-        return [
-            remote(
-                PS.at[b, q, span], PR.at[b, q], ps_.at[b, q], pr_.at[b, q], mate
-            )
-            for q in range(4)
-        ]
-
-    def down(b):
-        sends = half_sends(b)
-        for q in range(4):
-            for p in range(nz):
-                wide = jnp.concatenate([DW[b, p, 0], DW[b, p, 1]], axis=1)
-                PS[b, q, p] = jnp.dot(
-                    H[q * rows:(q + 1) * rows, :], wide, preferred_element_type=F32
-                ).astype(BF16)
-            sends[q].start()
-
-    def sum_half(b, q):
-        for i in range(nz // 2):
-            mine = PS[b, q, t * (nz // 2) + i].astype(F32)
-            S[b, q, :, i * 2 * cw:(i + 1) * 2 * cw] = (mine + PR[b, q, i].astype(F32)).astype(BF16)
+        return [half_send(b, i) for i in range(4)]
+
+    def down(b, i):
+        q = turn[i]
+        for p in range(nz):
+            wide = jnp.concatenate([DW[b, p, 0], DW[b, p, 1]], axis=1)
+            PS[b, q, p] = jnp.dot(H[rows_of(q), :], wide, preferred_element_type=F32).astype(BF16)
+        half_send(b, i).start()
+
+    def quad_send(b, j):
+        return remote(S.at[b, quad_idx[j]], R.at[b, j], qs.at[b, j], qr.at[b, j], quad[j])
 
     def quad_sends(b):
-        return [
-            remote(S.at[b, quad_idx[j]], R.at[b, j], qs.at[b, j], qr.at[b, j], quad[j])
-            for j in range(3)
-        ]
-
-    def scatter(b):
-        sends = half_sends(b)
-        for q in range(4):
-            sends[q].wait_recv()
-            sum_half(b, q)
-        for j in (2, 1, 0):
-            quad_sends(b)[j].start()
+        return [quad_send(b, j) for j in range(3)]
+
+    def sum_half(b, i):
+        half_send(b, i).wait_recv()
+        q = turn[i]
+        for k in range(nz // 2):
+            mine = PS[b, q, t * (nz // 2) + k].astype(F32)
+            S[b, q, :, k * 2 * cw:(k + 1) * 2 * cw] = (mine + PR[b, q, k].astype(F32)).astype(BF16)
+        if i < 3:
+            quad_send(b, turn_peer[i]).start()
+
+    def project(b, prepare):
+        for i in range(4):
+            prepare(turn[i])
+            hidden_of(turn[i])
+            down(b, i)
+            if i:
+                sum_half(b, i - 1)
+        sum_half(b, 3)
+
+    def chunk(b, i, q, fresh):
+        p = order(i)
+        value = jnp.dot(N[p, rows_of(q), :], GU[b, p], preferred_element_type=F32)
+        if fresh:
+            ACC[rows_of(q), :] = value
+        else:
+            ACC[rows_of(q), :] += value
 
     def collect(b):
         for send in quad_sends(b):
             send.wait_recv()
         total = S[b, me].astype(F32)
-        for j in range(3):
+        for j in (2, 0, 1):
             total = total + R[b, j].astype(F32)
         return total
 
+    for b in range(2):
+        for c in tail_loads(b):
+            c.start()
+    T[0, me, t] = tok_ref[...]
+    for b in range(2):
+        tail_make(b)
     for c in own_copies(0):
         c.start()
-    T[0, me, t] = tok_ref[...]
     pl.semaphore_wait(
         barrier, 4 + jnp.minimum(z, 1) + jnp.minimum(nz - 1 - z, 1)
     )
@@ -393,9 +426,7 @@
                 c.wait_recv()
             z_send(1, 0, 0)
             z_send(1, 0, 1)
-    hidden_of()
-    down(0)
-    scatter(0)
+    project(0, lambda q: None)
     z_take(0, nz - 2, 2)
     z_take(1, 0, 0)
     z_take(1, 0, 1)
@@ -441,21 +472,20 @@
     z_take(1, 1, 1)
     mate_own(1).wait_recv()
     norm_block(1, me, post_ref)
+    for i in range(nz - 1):
+        chunk(1, i, me, i == 0)
     for j in (0, 2, 1):
         tok_sends(1)[j].wait_recv()
         mate_pass(1, j).start()
     for j in (0, 2, 1):
         mate_pass(1, j).wait_recv()
         norm_block(1, quad_idx[j], post_ref)
-    for i in range(nz - 1):
-        gate_up(1, i)
+        for i in range(nz - 1):
+            chunk(1, i, quad_idx[j], i == 0)
     for k in range(2, nz - 1):
         z_take(1, k, 0)
         z_take(1, k, 1)
-    gate_up(1, nz - 1)
-    hidden_of()
-    down(1)
-    scatter(1)
+    project(1, lambda q: chunk(1, nz - 1, q, False))
     out_ref[...] = (T[1, me, t].astype(F32) + 0.5 * collect(1)).astype(BF16)
 
     for b in range(2):
@@ -481,10 +511,6 @@
     rest = hid // 4 - main
     groups, width, out_cols = pool_weight.shape
 
-    def tail_of(gate, up):
-        parts = [v[:, 4 * main:].reshape(depth, 4, rest) for v in (gate, up)]
-        return jnp.concatenate(parts, axis=2).reshape(depth, 8 * rest)
-
     vmem = pl.BlockSpec(memory_space=pltpu.VMEM)
     anyw = pl.BlockSpec(memory_space=pl.ANY)
     dma = pltpu.SemaphoreType.DMA
@@ -493,7 +519,7 @@
     out = pl.pallas_call(
         functools.partial(layer_kernel, nz),
         out_shape=jax.ShapeDtypeStruct((rows, half), BF16),
-        in_specs=[vmem] * 6 + [anyw] * 8,
+        in_specs=[vmem] * 6 + [anyw] * 6,
         out_specs=vmem,
         scratch_shapes=[
             pltpu.VMEM((2, nz, 2 * depth, big), BF16),
@@ -508,6 +534,9 @@
             pltpu.VMEM((2, 4, rows, half), BF16),
             pltpu.VMEM((2, 3, rows, half), BF16),
             pltpu.VMEM((2, rows, 128), F32),
+            pltpu.VMEM((2, 2, depth, 4 * rest), BF16),
+            pltpu.VMEM((2, depth, 8 * rest), BF16),
+            dma((2, 2)),
             dma((2, 6)), dma((2, 6)), dma((2, 6)),
             dma((2, 2, steps, 3)), dma((2, 2, steps, 3)),
             dma((2, 3)), dma((2, 3)), dma((2, 3)), dma((2, 3)),
@@ -519,7 +548,6 @@
     )(
         tokens.reshape(rows, half), pre_gain.reshape(1, -1), mix_gain.reshape(1, -1),
         pool_scale.reshape(1, -1), post_gain.reshape(1, -1), jnp.swapaxes(pool_weight, 1, 2),
-        tail_of(first_gate, first_up), tail_of(second_gate, second_up),
         first_gate, first_up, first_down, second_gate, second_up, second_down,
     )
     return out.reshape(tokens.shape)

time: 117 us -> 106 us (0.906)
  local copies, waits for them, and re-layouts: 7 us -> 1.67 us
  Pallas kernels: 110 us -> 105 us
    pallas_call x1, Pallas kernels: 110 us -> 105 us  [fused(): pl.pallas_call(functools.partial(layer_kernel, nz), out_shape=jax.ShapeDt...]
    slice x8 -> x0, local copies, waits for them, and re-layouts: 3.35 us -> none  [tail_of(): parts = [v[:, 4 * main:].reshape(depth, 4, rest) for v in (gate, up)]]
    reshape x2 -> x0, local copies, waits for them, and re-layouts: 1.54 us -> none  [tail_of(): return jnp.concatenate(parts, axis=2).reshape(depth, 8 * rest)]
where the time goes in v2:
time: 106 us
  Pallas kernels  105 us (99%)
  local copies, waits for them, and re-layouts  1.67 us (2%)
    pallas_call x1, Pallas kernels, fused(): pl.pallas_call(functools.partial(layer_kernel, nz), out_shape=jax.ShapeDt...  105 us

profile of v2, /device:TPU:0, one launch (start us, length us, event | category | flops | bytes accessed | tf_op | source)
XLA Modules:
  0.0 106.2 jit_solution(9550913319798519206)
XLA Ops:
  0.0 104.6 %shard_map.118 = bf16[256,512]{1,0:T(8,128)(2,1)} custom-call(bf16[256,512]{1,0:T(8,128)(2,1)} %bitcast.8, f32[1,1024]{1,0:T(1,128)} %bitcast.10, f32[1,512]{1,0:T(1,128)} %bitcast.12, f32[1,512]{1,0:T(1,128)} %bitcast.13, f32[1,1024]{1,0:T(1,128)} %bitcast.11, bf16[2,32,256]{2,1,0:T(8,128)(2,1)} %bitcast.9, bf16[128,1280]{1,0:T(8,128)(2,1)} %g1_ref.1, ...), custom_call_target="tpu_custom_call" | custom-call | tf_op jit(solution)/shard_map/pallas_call | solution.py:519
  104.6 1.7 %copy.14 = bf16[1,256,512]{2,1,0:T(8,128)(2,1)} copy(bf16[1,256,512]{2,1,0:T(8,128)(2,1)} %bitcast.7) | data formatting | bytes 524288

commit v3 on v2

--- a/solution.py
+++ b/solution.py
@@ -250,17 +250,30 @@
         def _():
             z_down(b, k, kind).wait_send()
 
+    def z_pass(b, k, kind):
+        @pl.when(jnp.logical_and(z - 1 - k >= 0, has_above))
+        def _():
+            z_up(b, k, kind).wait_recv()
+            z_up(b, k + 1, kind).start()
+
+        @pl.when(jnp.logical_and(z + 1 + k <= nz - 1, has_below))
+        def _():
+            z_down(b, k, kind).wait_recv()
+            z_down(b, k + 1, kind).start()
+
+    def z_end(b, k, kind):
+        @pl.when(jnp.logical_and(z - 1 - k >= 0, z == nz - 1))
+        def _():
+            z_up(b, k, kind).wait_recv()
+
+        @pl.when(jnp.logical_and(z + 1 + k <= nz - 1, z == 0))
+        def _():
+            z_down(b, k, kind).wait_recv()
+
     def z_take(b, k, kind):
-        @pl.when(z - 1 - k >= 0)
-        def _():
-            z_up(b, k, kind).wait_recv()
-
-        @pl.when(z + 1 + k <= nz - 1)
-        def _():
-            z_down(b, k, kind).wait_recv()
-
         if k + 1 < nz - 1:
-            z_send(b, k + 1, kind)
+            z_pass(b, k, kind)
+        z_end(b, k, kind)
 
     def tok_sends(b):
         mine = T.at[b, me, t]
@@ -349,7 +362,6 @@
     def project(b, prepare):
         for i in range(4):
             prepare(turn[i])
-            hidden_of(turn[i])
             down(b, i)
             if i:
                 sum_half(b, i - 1)
@@ -426,10 +438,11 @@
                 c.wait_recv()
             z_send(1, 0, 0)
             z_send(1, 0, 1)
-    project(0, lambda q: None)
+    project(0, hidden_of)
     z_take(0, nz - 2, 2)
-    z_take(1, 0, 0)
-    z_take(1, 0, 1)
+    for k in range(nz - 2):
+        z_pass(1, k, 0)
+        z_pass(1, k, 1)
     first = collect(0)
     after_first = (tok_ref[...].astype(F32) + 0.5 * first).astype(BF16).astype(F32)
     square = after_first * after_first
@@ -468,8 +481,8 @@
     for j in (0, 2, 1):
         tok_sends(1)[j].start()
     mate_own(1).start()
-    z_take(1, 1, 0)
-    z_take(1, 1, 1)
+    for k in range(nz - 2):
+        z_end(1, k, 0)
     mate_own(1).wait_recv()
     norm_block(1, me, post_ref)
     for i in range(nz - 1):
@@ -482,10 +495,13 @@
         norm_block(1, quad_idx[j], post_ref)
         for i in range(nz - 1):
             chunk(1, i, quad_idx[j], i == 0)
-    for k in range(2, nz - 1):
-        z_take(1, k, 0)
-        z_take(1, k, 1)
-    project(1, lambda q: chunk(1, nz - 1, q, False))
+    z_end(1, nz - 2, 0)
+    for q in turn:
+        chunk(1, nz - 1, q, False)
+        hidden_of(q)
+    for k in range(nz - 1):
+        z_end(1, k, 1)
+    project(1, lambda q: None)
     out_ref[...] = (T[1, me, t].astype(F32) + 0.5 * collect(1)).astype(BF16)
 
     for b in range(2):

time: 106 us -> 107 us (level)
  no operation moved by 1% of the time
where the time goes in v3:
time: 107 us
  Pallas kernels  105 us (98%)
  local copies, waits for them, and re-layouts  1.67 us (2%)
    pallas_call x1, Pallas kernels, fused(): pl.pallas_call(functools.partial(layer_kernel, nz), out_shape=jax.ShapeDt...  105 us

profile of v3, /device:TPU:0, one launch (start us, length us, event | category | flops | bytes accessed | tf_op | source)
XLA Modules:
  0.0 107.1 jit_solution(2096770747307059352)
XLA Ops:
  0.0 105.4 %shard_map.118 = bf16[256,512]{1,0:T(8,128)(2,1)} custom-call(bf16[256,512]{1,0:T(8,128)(2,1)} %bitcast.8, f32[1,1024]{1,0:T(1,128)} %bitcast.10, f32[1,512]{1,0:T(1,128)} %bitcast.12, f32[1,512]{1,0:T(1,128)} %bitcast.13, f32[1,1024]{1,0:T(1,128)} %bitcast.11, bf16[2,32,256]{2,1,0:T(8,128)(2,1)} %bitcast.9, bf16[128,1280]{1,0:T(8,128)(2,1)} %g1_ref.1, ...), custom_call_target="tpu_custom_call" | custom-call | tf_op jit(solution)/shard_map/pallas_call | solution.py:535
  105.4 1.7 %copy.14 = bf16[1,256,512]{2,1,0:T(8,128)(2,1)} copy(bf16[1,256,512]{2,1,0:T(8,128)(2,1)} %bitcast.7) | data formatting | bytes 524288
